TPU v7x, 256 devices: a whole 4x4x8 slice. The times are simulated.
256 devices in a mesh: fs: 32 (over z, x), tp: 8 (over y, core).
Axes of the slice: x: 4, y: 4, z: 8, core: 2. Of those that a mesh axis runs over, the one named last changes fastest.
Arguments:
- tokens: bfloat16 [16384, 2048], P('fs', 'tp'), may hold values from -6 to 6
- pre_gain: float32 [2048], replicated, may hold values from 0.1 to 1.9
- pre_gate: float32 [2048, 2816], P('fs', 'tp'), may hold values from -0.125 to 0.125
- pre_up: float32 [2048, 2816], P('fs', 'tp'), may hold values from -0.125 to 0.125
- pre_down: float32 [2816, 2048], P('fs', 'tp'), may hold values from -0.109375 to 0.109375
- mix_gain: float32 [2048], replicated, may hold values from 0.1 to 1.9
- branch_proj: float32 [2048, 1024], P('fs', 'tp'), may hold values from -0.125 to 0.125
- gate_proj: float32 [2048, 1024], P('fs', 'tp'), may hold values from -0.125 to 0.125
- conv_taps: float32 [4, 1024], P(None, 'tp'), may hold values from -3 to 3
- retain_blocks: float32 [16, 64, 64], P('tp'), may hold values from -0.75 to 0.75
- admit_blocks: float32 [16, 64, 64], P('tp'), may hold values from -0.75 to 0.75
- decay_param: float32 [1024], P('tp'), may hold values from 5 to 8.5
- channel_gain: float32 [1024], replicated, may hold values from 0.1 to 1.9
- out_proj: float32 [1024, 2048], P('fs', 'tp'), may hold values from -0.1875 to 0.1875
- post_gain: float32 [2048], replicated, may hold values from 0.1 to 1.9
- post_gate: float32 [2048, 2816], P('fs', 'tp'), may hold values from -0.125 to 0.125
- post_up: float32 [2048, 2816], P('fs', 'tp'), may hold values from -0.125 to 0.125
- post_down: float32 [2816, 2048], P('fs', 'tp'), may hold values from -0.109375 to 0.109375
Outputs:
- layer_out: bfloat16 [16384, 2048], P('fs', 'tp')
All inputs are finite; a program needn't handle non-finite values.
Results may differ from a plain program's by a relative error of at most 0.012.
Values may be sent and summed in bfloat16 or wider, within the bound.
A program may use at most 64 MiB of HBM per device.

v0:
```python
import jax
import jax.numpy as jnp
from jax import lax
from jax.sharding import Mesh
from jax.sharding import PartitionSpec as P

SEQ_LEN = 128
FS = ("fs_0", "fs_1")
EPSILON = 1e-06
DECAY_SCALE = 8.0


def copy_for_each(x, axis):
    copies = jnp.broadcast_to(x, (lax.axis_size(axis), *x.shape))
    return lax.all_to_all(copies, axis, split_axis=0, concat_axis=0, tiled=True)


def laid_out(parts, dim):
    dims = list(parts.shape[1:])
    dims[dim] *= parts.shape[0]
    return jnp.moveaxis(parts, 0, dim).reshape(dims)


def gather_directly(x, axis, dim):
    parts = copy_for_each(x, axis)
    return laid_out(parts, dim)


def gathered_by_axis(x, axes, dim):
    whole = x
    for number in range(len(axes) - 1, -1, -1):
        whole = lax.all_gather(whole, axes[number], axis=dim, tiled=True)
    return whole


def normalize(values, norm_gain):
    floats = values.astype(jnp.float32)
    scaled = floats * lax.rsqrt(jnp.mean(floats * floats, axis=-1, keepdims=True) + EPSILON)
    return (scaled * norm_gain).astype(jnp.bfloat16)


def combine(earlier, latter):
    keep_early, add_early = earlier
    keep_late, add_late = latter
    return (keep_early * keep_late, keep_late * add_early + add_late)


def widen(residual):
    return gather_directly(residual, "tp", 1)


def contract(operand, stacked):
    return jnp.dot(
        operand,
        gathered_by_axis(stacked.astype(jnp.bfloat16), FS, 0),
        preferred_element_type=jnp.float32,
    )


def feed_forward(residual, norm_gain, gate_matrix, up_matrix, down_matrix):
    normed = normalize(widen(residual), norm_gain)
    products = contract(normed, jnp.concatenate((gate_matrix, up_matrix), axis=1))
    split_at = gate_matrix.shape[1]
    hidden = (jax.nn.silu(products[:, :split_at]) * products[:, split_at:]).astype(jnp.bfloat16)
    all_hidden = lax.all_gather(hidden, "tp", axis=1, tiled=True)
    return (residual.astype(jnp.float32) + 0.5 * contract(all_hidden, down_matrix)).astype(
        jnp.bfloat16
    )


def block_gate(convolved, blocks):
    grouped = convolved.reshape(
        convolved.shape[0], convolved.shape[1], blocks.shape[0], blocks.shape[1]
    )
    mixed = jnp.einsum(
        "sthi,hij->sthj", grouped, blocks.astype(jnp.bfloat16), preferred_element_type=jnp.float32
    )
    return jax.nn.sigmoid(mixed).reshape(convolved.shape)


def recurrent_mixer(
    residual,
    norm_gain,
    branch_matrix,
    gate_matrix,
    conv_taps,
    retain_blocks,
    admit_blocks,
    decay_param,
    channel_gain,
    out_matrix,
):
    normed = normalize(widen(residual), norm_gain)
    products = contract(normed, jnp.concatenate((branch_matrix, gate_matrix), axis=1))
    local_width = branch_matrix.shape[1]
    branch = products[:, :local_width]
    gate_act = products[:, local_width:]
    taps_count = conv_taps.shape[0]
    sequences = residual.shape[0] // SEQ_LEN
    framed = branch.reshape(sequences, SEQ_LEN, local_width)
    padded = jnp.pad(framed, ((0, 0), (taps_count - 1, 0), (0, 0)))
    convolved = jnp.zeros_like(framed)
    for tap_index in range(taps_count):
        convolved = convolved + padded[:, tap_index : tap_index + SEQ_LEN] * conv_taps[tap_index]
    convolved = convolved.astype(jnp.bfloat16)
    retained = block_gate(convolved, retain_blocks)
    admitted = block_gate(convolved, admit_blocks)
    log_keep = -DECAY_SCALE * retained * jax.nn.softplus(-decay_param)
    inject = jnp.sqrt(-jnp.expm1(2.0 * log_keep)) * admitted * convolved.astype(jnp.float32)
    _, states = lax.associative_scan(combine, (jnp.exp(log_keep), inject), axis=1)
    mixed_rows = (states.reshape(residual.shape[0], local_width) * jax.nn.gelu(gate_act)).astype(
        jnp.bfloat16
    )
    all_channels = gather_directly(mixed_rows, "tp", 1)
    mixed_normed = normalize(all_channels, channel_gain)
    return (residual.astype(jnp.float32) + contract(mixed_normed, out_matrix)).astype(jnp.bfloat16)


def local(
    tokens,
    pre_gain,
    pre_gate,
    pre_up,
    pre_down,
    mix_gain,
    branch_proj,
    gate_proj,
    conv_taps,
    retain_blocks,
    admit_blocks,
    decay_param,
    channel_gain,
    out_proj,
    post_gain,
    post_gate,
    post_up,
    post_down,
):
    after_pre = feed_forward(tokens, pre_gain, pre_gate, pre_up, pre_down)
    after_mix = recurrent_mixer(
        after_pre,
        mix_gain,
        branch_proj,
        gate_proj,
        conv_taps,
        retain_blocks,
        admit_blocks,
        decay_param,
        channel_gain,
        out_proj,
    )
    return feed_forward(after_mix, post_gain, post_gate, post_up, post_down)


def solution(mesh):
    torus = Mesh(mesh.devices.reshape(8, 4, mesh.shape["tp"]), ("fs_0", "fs_1", "tp"))
    placed = (
        P(FS, "tp"),
        P(),
        P(FS, "tp"),
        P(FS, "tp"),
        P(FS, "tp"),
        P(),
        P(FS, "tp"),
        P(FS, "tp"),
        P(None, "tp"),
        P("tp", None, None),
        P("tp", None, None),
        P("tp"),
        P(),
        P(FS, "tp"),
        P(),
        P(FS, "tp"),
        P(FS, "tp"),
        P(FS, "tp"),
    )
    return jax.shard_map(local, mesh=torus, in_specs=placed, out_specs=P(FS, "tp"), check_vma=False)
```

profile of v0, /device:TPU:1, one launch (start us, length us, event | category | flops | bytes accessed | tf_op | source)
XLA Modules:
  0.0 431.4 jit_solution(11646481140543656673)
XLA Ops:
  8.4 12.3 %all_gather.42 = bf16[256,704]{1,0:T(8,128)(2,1)} all-gather(bf16[64,704]{1,0:T(8,128)(2,1)S(1)} %pad_maximum_fusion.3), channel_id=1, replica_groups=mesh['fs_0'=8,'fs_1'=4,'tp'=8] {'fs_1'}, dimensions={0}, use_global_device_ids=true | all-gather | bytes 450560 | tf_op jit(solution)/shard_map/all_gather | solution.py:32
  23.4 8.2 %all-to-all-start = ((bf16[8,512,256]{1,2,0:T(8,128)(2,1)}), bf16[8,512,256]{1,2,0:T(8,128)(2,1)S(1)}, u32[]{:S(2)}, u32[]{:S(2)}) async-start(bf16[8,512,256]{1,2,0:T(8,128)(2,1)} %broadcast_in_dim.8), calls=%async_computation | async-start | bytes 4194304 | tf_op jit(solution)/shard_map/all_to_all | solution.py:15
  31.6 10.6 %all_gather.45 = bf16[352,256]{1,0:T(8,128)(2,1)} all-gather(bf16[88,256]{1,0:T(8,128)(2,1)S(1)} %convert_element_type.124), channel_id=1, replica_groups=mesh['fs_0'=8,'fs_1'=4,'tp'=8] {'fs_1'}, dimensions={0}, use_global_device_ids=true | all-gather | bytes 225280 | tf_op jit(solution)/shard_map/all_gather | solution.py:32
  42.2 15.5 %all-to-all-done = bf16[8,512,256]{1,2,0:T(8,128)(2,1)S(1)} async-done(((bf16[8,512,256]{1,2,0:T(8,128)(2,1)}), bf16[8,512,256]{1,2,0:T(8,128)(2,1)S(1)}, u32[]{:S(2)}, u32[]{:S(2)}) %all-to-all-start) | async-done | bytes 2097184 | tf_op jit(solution)/shard_map/all_to_all | solution.py:15
  60.2 10.1 %all-gather.8.cloned.1.call-done = bf16[2048,704]{1,0:T(8,128)(2,1)} async-done(((bf16[256,704]{1,0:T(8,128)(2,1)}), bf16[2048,704]{1,0:T(8,128)(2,1)}) %all-gather.8.cloned.1.call-update) | async-done | bytes 2883600 | tf_op jit(solution)/shard_map/all_gather | solution.py:32
  70.3 4.2 fusion.56
  75.6 10.4 %all_gather.47 = bf16[256,256]{1,0:T(8,128)(2,1)} all-gather(bf16[64,256]{1,0:T(8,128)(2,1)S(1)} %pad_maximum_fusion.5), channel_id=1, replica_groups=mesh['fs_0'=8,'fs_1'=4,'tp'=8] {'fs_1'}, dimensions={0}, use_global_device_ids=true | all-gather | bytes 163840 | tf_op jit(solution)/shard_map/all_gather | solution.py:32
  86.1 20.4 %all-gather.12.cloned.1.call-done = bf16[2816,256]{1,0:T(8,128)(2,1)} async-done(((bf16[352,256]{1,0:T(8,128)(2,1)}), bf16[2816,256]{1,0:T(8,128)(2,1)}) %all-gather.12.cloned.1.call-update) | async-done | bytes 1441808 | tf_op jit(solution)/shard_map/all_gather | solution.py:32
  106.5 34.1 %all-gather.10.cloned.1.call-done = bf16[512,2816]{0,1:T(8,128)(2,1)} async-done(((bf16[512,352]{0,1:T(8,128)(2,1)}), bf16[512,2816]{0,1:T(8,128)(2,1)}) %all-gather.10.cloned.1.call-update) | async-done | bytes 2883600 | tf_op jit(solution)/shard_map/all_gather | solution.py:65
  140.6 3.2 fusion.12
  145.5 3.9 all-to-all-start.1
  149.5 11.1 %all_gather.51 = bf16[256,704]{1,0:T(8,128)(2,1)} all-gather(bf16[64,704]{1,0:T(8,128)(2,1)S(1)} %pad_maximum_fusion.4), channel_id=1, replica_groups=mesh['fs_0'=8,'fs_1'=4,'tp'=8] {'fs_1'}, dimensions={0}, use_global_device_ids=true | all-gather | bytes 450560 | tf_op jit(solution)/shard_map/all_gather | solution.py:32
  160.7 15.0 %all-to-all-done.1 = bf16[8,512,256]{1,2,0:T(8,128)(2,1)S(1)} async-done(((bf16[8,512,256]{1,2,0:T(8,128)(2,1)}), bf16[8,512,256]{1,2,0:T(8,128)(2,1)S(1)}, u32[]{:S(2)}, u32[]{:S(2)}) %all-to-all-start.1) | async-done | bytes 2097184 | tf_op jit(solution)/shard_map/all_to_all | solution.py:15
  178.0 2.6 fusion.57
  182.9 4.9 %slice.212 = f32[4,64,128]{1,2,0:T(8,128)S(1)} slice(f32[4,128,128]{1,2,0:T(8,128)S(1)} %get-tuple-element.6), slice={[0:4:1], [0:127:2], [0:128:1]} | slice | bytes 262144 | tf_op jit(solution)/shard_map/slice | solution.py:110
  187.9 4.5 %slice.213 = f32[4,64,128]{1,2,0:T(8,128)S(1)} slice(f32[4,128,128]{1,2,0:T(8,128)S(1)} %get-tuple-element.6), slice={[0:4:1], [1:128:2], [0:128:1]} | slice | bytes 262144 | tf_op jit(solution)/shard_map/slice | solution.py:110
  192.4 4.5 %slice.211 = f32[4,64,128]{1,2,0:T(8,128)S(1)} slice(f32[4,128,128]{1,2,0:T(8,128)S(1)} %get-tuple-element.5), slice={[0:4:1], [1:128:2], [0:128:1]} | slice | bytes 262144 | tf_op jit(solution)/shard_map/slice | solution.py:110
  197.0 4.5 %slice.215 = f32[4,64,128]{1,2,0:T(8,128)S(1)} slice(f32[4,128,128]{1,2,0:T(8,128)S(1)} %get-tuple-element.5), slice={[0:4:1], [0:127:2], [0:128:1]} | slice | bytes 262144 | tf_op jit(solution)/shard_map/slice | solution.py:110
  245.6 4.5 %slice.259 = f32[4,63,128]{1,2,0:T(8,128)S(1)} slice(f32[4,128,128]{1,2,0:T(8,128)S(1)} %get-tuple-element.6), slice={[0:4:1], [2:128:2], [0:128:1]} | slice | bytes 258048 | tf_op jit(solution)/shard_map/slice | solution.py:110
  250.1 4.5 %slice.210 = f32[4,63,128]{1,2,0:T(8,128)S(1)} slice(f32[4,128,128]{1,2,0:T(8,128)S(1)} %get-tuple-element.5), slice={[0:4:1], [2:128:2], [0:128:1]} | slice | bytes 258048 | tf_op jit(solution)/shard_map/slice | solution.py:110
  276.4 4.6 %pad.61 = f32[4,128,128]{1,2,0:T(8,128)S(1)} pad(f32[4,64,128]{1,2,0:T(8,128)S(1)} %add.195, f32[]{:T(128)} %constant.10.clone.1), padding=0_0_0x1_0_1x0_0_0 | pad | bytes 393220 | tf_op jit(solution)/shard_map/pad | solution.py:110
  281.2 4.5 %pad.60 = f32[4,128,128]{1,2,0:T(8,128)S(1)} pad(f32[4,64,128]{1,2,0:T(8,128)S(1)} %pad_maximum_fusion.2, f32[]{:T(128)} %constant.10.clone.1), padding=0_0_0x0_1_1x0_0_0 | pad | bytes 393220 | tf_op jit(solution)/shard_map/pad | solution.py:110
  287.3 7.7 %all-to-all-start.2 = ((bf16[8,512,128]{1,2,0:T(8,128)(2,1)}), bf16[8,512,128]{1,2,0:T(8,128)(2,1)S(1)}, u32[]{:S(2)}, u32[]{:S(2)}) async-start(bf16[8,512,128]{1,2,0:T(8,128)(2,1)} %broadcast_in_dim.10), calls=%async_computation.2 | async-start | bytes 2097152 | tf_op jit(solution)/shard_map/all_to_all | solution.py:15
  295.0 10.3 %all_gather.49 = bf16[128,256]{1,0:T(8,128)(2,1)S(1)} all-gather(bf16[32,256]{1,0:T(8,128)(2,1)S(1)} %convert_element_type.142), channel_id=1, replica_groups=mesh['fs_0'=8,'fs_1'=4,'tp'=8] {'fs_1'}, dimensions={0}, use_global_device_ids=true | all-gather | bytes 81920 | tf_op jit(solution)/shard_map/all_gather | solution.py:32
  305.3 20.3 %all_gather.50 = bf16[1024,256]{1,0:T(8,128)(2,1)S(1)} all-gather(bf16[128,256]{1,0:T(8,128)(2,1)S(1)} %all_gather.49), channel_id=1, replica_groups=mesh['fs_0'=8,'fs_1'=4,'tp'=8] {'fs_0'}, dimensions={0}, use_global_device_ids=true | all-gather | bytes 589824 | tf_op jit(solution)/shard_map/all_gather | solution.py:32
  328.3 12.1 %all-to-all-start.3 = ((bf16[8,512,256]{1,2,0:T(8,128)(2,1)}), bf16[8,512,256]{1,2,0:T(8,128)(2,1)S(1)}, u32[]{:S(2)}, u32[]{:S(2)}) async-start(bf16[8,512,256]{1,2,0:T(8,128)(2,1)} %broadcast_in_dim.11), calls=%async_computation.3 | async-start | bytes 4194304 | tf_op jit(solution)/shard_map/all_to_all | solution.py:15
  340.5 10.3 %all_gather.54 = bf16[352,256]{1,0:T(8,128)(2,1)} all-gather(bf16[88,256]{1,0:T(8,128)(2,1)S(1)} %convert_element_type.151), channel_id=1, replica_groups=mesh['fs_0'=8,'fs_1'=4,'tp'=8] {'fs_1'}, dimensions={0}, use_global_device_ids=true | all-gather | bytes 225280 | tf_op jit(solution)/shard_map/all_gather | solution.py:32
  350.9 15.8 %all-to-all-done.3 = bf16[8,512,256]{1,2,0:T(8,128)(2,1)S(1)} async-done(((bf16[8,512,256]{1,2,0:T(8,128)(2,1)}), bf16[8,512,256]{1,2,0:T(8,128)(2,1)S(1)}, u32[]{:S(2)}, u32[]{:S(2)}) %all-to-all-start.3) | async-done | bytes 2097184 | tf_op jit(solution)/shard_map/all_to_all | solution.py:15
  369.0 4.3 fusion.58
  374.3 11.7 %all-gather.20.cloned.1.call-done = bf16[2816,256]{1,0:T(8,128)(2,1)} async-done(((bf16[352,256]{1,0:T(8,128)(2,1)}), bf16[2816,256]{1,0:T(8,128)(2,1)}) %all-gather.20.cloned.1.call-update) | async-done | bytes 1441808 | tf_op jit(solution)/shard_map/all_gather | solution.py:32
  386.0 34.4 %all-gather.18.cloned.1.call-done = bf16[512,2816]{0,1:T(8,128)(2,1)} async-done(((bf16[512,352]{0,1:T(8,128)(2,1)}), bf16[512,2816]{0,1:T(8,128)(2,1)}) %all-gather.18.cloned.1.call-update) | async-done | bytes 2883600 | tf_op jit(solution)/shard_map/all_gather | solution.py:65
  420.4 3.9 fusion.11
  (187 shorter events, 87.9 us)
Async XLA Ops:
  6.5 63.8 %all-gather.8.cloned.1.call-start = ((), (), s32[]{:S(2)}) async-start(), calls=%async_computation.4 | async-start | bytes 3538944 | tf_op jit(solution)/shard_map/all_gather | solution.py:32
  23.4 8.2 %copy-start.9 = (f32[88,256]{1,0:T(8,128)S(1)}, f32[88,256]{1,0:T(8,128)}, u32[]{:S(2)}) copy-start(f32[88,256]{1,0:T(8,128)} %param.22) | copy-start | bytes 270340
  23.4 34.4 %all-to-all-start = ((bf16[8,512,256]{1,2,0:T(8,128)(2,1)}), bf16[8,512,256]{1,2,0:T(8,128)(2,1)S(1)}, u32[]{:S(2)}, u32[]{:S(2)}) async-start(bf16[8,512,256]{1,2,0:T(8,128)(2,1)} %broadcast_in_dim.8), calls=%async_computation | async-start | bytes 4194304 | tf_op jit(solution)/shard_map/all_to_all | solution.py:15
  31.5 26.8 %copy-start.14 = (f32[2048]{0:T(1024)S(1)}, f32[2048]{0:T(1024)}, u32[]{:S(2)}) copy-start(f32[2048]{0:T(1024)} %param.19) | copy-start | bytes 24580
  31.5 75.0 %all-gather.12.cloned.1.call-start = ((), (), s32[]{:S(2)}) async-start(), calls=%async_computation.6 | async-start | bytes 1622016 | tf_op jit(solution)/shard_map/all_gather | solution.py:32
  42.2 98.4 %all-gather.10.cloned.1.call-start = ((), (), s32[]{:S(2)}) async-start(), calls=%async_computation.5 | async-start | bytes 3244032 | tf_op jit(solution)/shard_map/all_gather | solution.py:65
  74.5 1.1 copy-start.11
  74.5 1.1 copy-start.12
  74.5 66.1 %copy-start.2 = (bf16[512,256]{1,0:T(8,128)(2,1)S(1)}, bf16[512,256]{1,0:T(8,128)(2,1)}, u32[]{:S(2)}) copy-start(bf16[512,256]{1,0:T(8,128)(2,1)} %param.18) | copy-start | bytes 786436
  75.5 102.5 %all-gather.14.cloned.1.call-start = ((), (), s32[]{:S(2)}) async-start(), calls=%async_computation.7 | async-start | bytes 1179648 | tf_op jit(solution)/shard_map/all_gather | solution.py:32
  143.8 1.7 copy-start.3
  145.4 4.0 copy-start.7
  145.4 4.0 copy-start.8
  145.4 15.2 %copy-start.21 = (f32[128]{0:T(128)S(1)}, f32[128]{0:T(128)}, u32[]{:S(2)}) copy-start(f32[128]{0:T(128)} %param.29) | copy-start | bytes 1540
  145.4 15.2 %copy-start.18 = (f32[4,128]{1,0:T(4,128)S(1)}, f32[4,128]{1,0:T(4,128)}, u32[]{:S(2)}) copy-start(f32[4,128]{1,0:T(4,128)} %param.26) | copy-start | bytes 6148
  145.5 30.2 %all-to-all-start.1 = ((bf16[8,512,256]{1,2,0:T(8,128)(2,1)}), bf16[8,512,256]{1,2,0:T(8,128)(2,1)S(1)}, u32[]{:S(2)}, u32[]{:S(2)}) async-start(bf16[8,512,256]{1,2,0:T(8,128)(2,1)} %broadcast_in_dim.9), calls=%async_computation.1 | async-start | bytes 4194304 | tf_op jit(solution)/shard_map/all_to_all | solution.py:15
  149.4 26.8 %copy-start.15 = (f32[2048]{0:T(1024)S(1)}, f32[2048]{0:T(1024)}, u32[]{:S(2)}) copy-start(f32[2048]{0:T(1024)} %param.23) | copy-start | bytes 24580
  149.4 219.7 %all-gather.16.cloned.1.call-start = ((), (), s32[]{:S(2)}) async-start(), calls=%async_computation.8 | async-start | bytes 3538944 | tf_op jit(solution)/shard_map/all_gather | solution.py:32
  178.0 3.9 copy-start.19
  180.6 1.6 copy-start.20
  262.5 7.2 %copy-start.5 = (f32[4,15,128]{1,2,0:T(8,128)S(1)}, f32[4,15,128]{1,2,0:T(8,128)}, u32[]{:S(2)}) copy-start(f32[4,15,128]{1,2,0:T(8,128)} %slice.222) | copy-start | bytes 92164
  262.6 7.2 %copy-start.6 = (f32[4,15,128]{1,2,0:T(8,128)S(1)}, f32[4,15,128]{1,2,0:T(8,128)}, u32[]{:S(2)}) copy-start(f32[4,15,128]{1,2,0:T(8,128)} %slice.255) | copy-start | bytes 92164
  281.0 4.9 %copy-start.1 = (f32[512,256]{1,0:T(8,128)S(1)}, f32[512,256]{1,0:T(8,128)}, u32[]{:S(2)}) copy-start(f32[512,256]{1,0:T(8,128)} %copy-done) | copy-start | bytes 1572868
  285.9 9.0 %copy-start.13 = (f32[32,256]{1,0:T(8,128)S(1)}, f32[32,256]{1,0:T(8,128)}, u32[]{:S(2)}) copy-start(f32[32,256]{1,0:T(8,128)} %param.31) | copy-start | bytes 98308
  287.3 38.6 %copy-start.17 = (f32[1024]{0:T(1024)S(1)}, f32[1024]{0:T(1024)}, u32[]{:S(2)}) copy-start(f32[1024]{0:T(1024)} %param.30) | copy-start | bytes 12292
  287.3 38.3 %all-to-all-start.2 = ((bf16[8,512,128]{1,2,0:T(8,128)(2,1)}), bf16[8,512,128]{1,2,0:T(8,128)(2,1)S(1)}, u32[]{:S(2)}, u32[]{:S(2)}) async-start(bf16[8,512,128]{1,2,0:T(8,128)(2,1)} %broadcast_in_dim.10), calls=%async_computation.2 | async-start | bytes 2097152 | tf_op jit(solution)/shard_map/all_to_all | solution.py:15
  295.0 31.2 %copy-start.4 = (bf16[512,256]{1,0:T(8,128)(2,1)S(1)}, bf16[512,256]{1,0:T(8,128)(2,1)}, u32[]{:S(2)}) copy-start(bf16[512,256]{1,0:T(8,128)(2,1)} %copy-done.3) | copy-start | bytes 786436
  328.3 12.1 %copy-start.10 = (f32[88,256]{1,0:T(8,128)S(1)}, f32[88,256]{1,0:T(8,128)}, u32[]{:S(2)}) copy-start(f32[88,256]{1,0:T(8,128)} %param.35) | copy-start | bytes 270340
  328.3 38.3 %all-to-all-start.3 = ((bf16[8,512,256]{1,2,0:T(8,128)(2,1)}), bf16[8,512,256]{1,2,0:T(8,128)(2,1)S(1)}, u32[]{:S(2)}, u32[]{:S(2)}) async-start(bf16[8,512,256]{1,2,0:T(8,128)(2,1)} %broadcast_in_dim.11), calls=%async_computation.3 | async-start | bytes 4194304 | tf_op jit(solution)/shard_map/all_to_all | solution.py:15
  340.4 26.7 %copy-start.16 = (f32[2048]{0:T(1024)S(1)}, f32[2048]{0:T(1024)}, u32[]{:S(2)}) copy-start(f32[2048]{0:T(1024)} %param.32) | copy-start | bytes 24580
  340.4 45.6 %all-gather.20.cloned.1.call-start = ((), (), s32[]{:S(2)}) async-start(), calls=%async_computation.10 | async-start | bytes 1622016 | tf_op jit(solution)/shard_map/all_gather | solution.py:32
  350.8 69.6 %all-gather.18.cloned.1.call-start = ((), (), s32[]{:S(2)}) async-start(), calls=%async_computation.9 | async-start | bytes 3244032 | tf_op jit(solution)/shard_map/all_gather | solution.py:65
  (1 other events, 0.8 us)
Sparse Core Ops, SparseCore 0:
  20.9 49.3 all-gather.7
  72.1 34.3 all-gather.11
  108.3 32.2 all-gather.9
  142.2 34.1 all-gather.13
  178.0 47.0 all-gather.15
  350.9 35.0 all-gather.19
  387.8 32.5 all-gather.17
where the time goes:
time: 439 us; the launch traced here: 431 us
  waiting for transfers between devices  157 us (36%)
  local copies, waits for them, and re-layouts  101 us (23%)
  blocking collectives  85.3 us (19%)
  starting transfers between devices  32 us (7%)
  other arithmetic  22 us (5%)
  matrix products  19.2 us (4%)
  between operations  14.6 us (3%)
    all_gather x7, blocking collectives, gathered_by_axis(): whole = lax.all_gather(whole, axes[number], axis=dim, tiled=True)  85.3 us
    all_gather x2, waiting for transfers between devices, feed_forward(): all_hidden = lax.all_gather(hidden, 'tp', axis=1, tiled=True)  68.5 us
    slice x34, local copies, waits for them, and re-layouts, recurrent_mixer(): lax.associative_scan(combine, (jnp.exp(log_keep), inject), axis=1)  65.6 us
    all_to_all x4, waiting for transfers between devices, copy_for_each(): return lax.all_to_all(copies, axis, split_axis=0, concat_axis=0, tiled=True)  46.2 us
    all_gather x5, waiting for transfers between devices, gathered_by_axis(): whole = lax.all_gather(whole, axes[number], axis=dim, tiled=True)  42.3 us
    all_to_all x4, starting transfers between devices, copy_for_each(): return lax.all_to_all(copies, axis, split_axis=0, concat_axis=0, tiled=True)  31.9 us
    pad x12, local copies, waits for them, and re-layouts, recurrent_mixer(): lax.associative_scan(combine, (jnp.exp(log_keep), inject), axis=1)  20.2 us
    dot_general x6, matrix products, contract(): jnp.dot(operand, gathered_by_axis(stacked.astype(jnp.bfloat16), FS, 0), p...  18.7 us
  transfers between devices with their start and end apart: 11, of which 8 were waited for; matrix products, arithmetic and copies ran while one was open for 31% of the time, Pallas kernels for 0%

commit v1 on v0

--- a/solution.py
+++ b/solution.py
@@ -62,7 +62,11 @@
     products = contract(normed, jnp.concatenate((gate_matrix, up_matrix), axis=1))
     split_at = gate_matrix.shape[1]
     hidden = (jax.nn.silu(products[:, :split_at]) * products[:, split_at:]).astype(jnp.bfloat16)
-    all_hidden = lax.all_gather(hidden, "tp", axis=1, tiled=True)
+    n_all = jax.lax.axis_size("tp")
+    sides = [n_all if b == 1 else 1 for b in range(hidden.ndim)]
+    all_hidden = jax.lax.all_to_all(
+        jnp.tile(hidden, sides), "tp", split_axis=1, concat_axis=1, tiled=True
+    )
     return (residual.astype(jnp.float32) + 0.5 * contract(all_hidden, down_matrix)).astype(
         jnp.bfloat16
     )

time: 439 us -> 405 us (0.923)
  waiting for transfers between devices: 157 us -> 115 us
  starting transfers between devices: 32 us -> 40.1 us
    all_gather x2 -> x0, waiting for transfers between devices: 68.5 us -> none  [feed_forward(): all_hidden = lax.all_gather(hidden, 'tp', axis=1, tiled=True)]
    all_to_all x0 -> x2, waiting for transfers between devices: none -> 38.5 us  [feed_forward(): jax.lax.all_to_all(jnp.tile(hidden, sides), 'tp', split_axis=1, concat_ax...]
    all_gather x5, waiting for transfers between devices: 42.3 us -> 30 us  [gathered_by_axis(): whole = lax.all_gather(whole, axes[number], axis=dim, tiled=True)]
    all_to_all x0 -> x2, starting transfers between devices: none -> 10.1 us  [feed_forward(): jax.lax.all_to_all(jnp.tile(hidden, sides), 'tp', split_axis=1, concat_ax...]
  transfers between devices with their start and end apart: 11 -> 11, of which waited for: 8 -> 8; matrix products, arithmetic and copies ran while one was open for 31% -> 34% of each run, Pallas kernels for 0% -> 0%
where the time goes in v1:
time: 405 us; the launch traced here: 397 us
  waiting for transfers between devices  115 us (28%)
  local copies, waits for them, and re-layouts  105 us (26%)
  blocking collectives  85.5 us (21%)
  starting transfers between devices  40.1 us (10%)
  other arithmetic  20.5 us (5%)
  matrix products  17.5 us (4%)
  between operations  14.2 us (4%)
    all_gather x7, blocking collectives, gathered_by_axis(): whole = lax.all_gather(whole, axes[number], axis=dim, tiled=True)  85.5 us
    slice x34, local copies, waits for them, and re-layouts, recurrent_mixer(): lax.associative_scan(combine, (jnp.exp(log_keep), inject), axis=1)  65.6 us
    all_to_all x4, waiting for transfers between devices, copy_for_each(): return lax.all_to_all(copies, axis, split_axis=0, concat_axis=0, tiled=True)  46 us
    all_to_all x2, waiting for transfers between devices, feed_forward(): jax.lax.all_to_all(jnp.tile(hidden, sides), 'tp', split_axis=1, concat_ax...  38.5 us
    all_gather x5, waiting for transfers between devices, gathered_by_axis(): whole = lax.all_gather(whole, axes[number], axis=dim, tiled=True)  30 us
    all_to_all x4, starting transfers between devices, copy_for_each(): return lax.all_to_all(copies, axis, split_axis=0, concat_axis=0, tiled=True)  30 us
    pad x12, local copies, waits for them, and re-layouts, recurrent_mixer(): lax.associative_scan(combine, (jnp.exp(log_keep), inject), axis=1)  20.2 us
    dot_general x6, matrix products, contract(): jnp.dot(operand, gathered_by_axis(stacked.astype(jnp.bfloat16), FS, 0), p...  16.9 us
  transfers between devices with their start and end apart: 11, of which 8 were waited for; matrix products, arithmetic and copies ran while one was open for 34% of the time, Pallas kernels for 0%

profile of v1, /device:TPU:1, one launch (start us, length us, event | category | flops | bytes accessed | tf_op | source)
XLA Modules:
  0.0 397.2 jit_solution(248016179326459989)
XLA Ops:
  8.4 12.3 %all_gather.36 = bf16[256,704]{1,0:T(8,128)(2,1)} all-gather(bf16[64,704]{1,0:T(8,128)(2,1)S(1)} %pad_maximum_fusion.3), channel_id=1, replica_groups=mesh['fs_0'=8,'fs_1'=4,'tp'=8] {'fs_1'}, dimensions={0}, use_global_device_ids=true | all-gather | bytes 450560 | tf_op jit(solution)/shard_map/all_gather | solution.py:32
  23.4 8.2 %all-to-all-start = ((bf16[8,512,256]{1,2,0:T(8,128)(2,1)}), bf16[8,512,256]{1,2,0:T(8,128)(2,1)S(1)}, u32[]{:S(2)}, u32[]{:S(2)}) async-start(bf16[8,512,256]{1,2,0:T(8,128)(2,1)} %broadcast_in_dim.8), calls=%async_computation | async-start | bytes 4194304 | tf_op jit(solution)/shard_map/all_to_all | solution.py:15
  31.5 10.6 %all_gather.38 = bf16[352,256]{1,0:T(8,128)(2,1)} all-gather(bf16[88,256]{1,0:T(8,128)(2,1)S(1)} %convert_element_type.124), channel_id=1, replica_groups=mesh['fs_0'=8,'fs_1'=4,'tp'=8] {'fs_1'}, dimensions={0}, use_global_device_ids=true | all-gather | bytes 225280 | tf_op jit(solution)/shard_map/all_gather | solution.py:32
  42.2 15.6 %all-to-all-done = bf16[8,512,256]{1,2,0:T(8,128)(2,1)S(1)} async-done(((bf16[8,512,256]{1,2,0:T(8,128)(2,1)}), bf16[8,512,256]{1,2,0:T(8,128)(2,1)S(1)}, u32[]{:S(2)}, u32[]{:S(2)}) %all-to-all-start) | async-done | bytes 2097184 | tf_op jit(solution)/shard_map/all_to_all | solution.py:15
  60.1 10.1 %all-gather.6.cloned.1.call-done = bf16[2048,704]{1,0:T(8,128)(2,1)} async-done(((bf16[256,704]{1,0:T(8,128)(2,1)}), bf16[2048,704]{1,0:T(8,128)(2,1)}) %all-gather.6.cloned.1.call-update) | async-done | bytes 2883600 | tf_op jit(solution)/shard_map/all_gather | solution.py:32
  70.3 4.2 %fusion.56 = f32[512,704]{0,1:T(8,128)S(1)} fusion(bf16[512,2048]{0,1:T(8,128)(2,1)} %fusion.5, bf16[2048,704]{1,0:T(8,128)(2,1)} %all-gather.6.cloned.1.call-done), kind=kOutput, calls=%fused_computation.110 | convolution fusion | flops 1476395008 | bytes 6422528 | tf_op jit(solution)/shard_map/dot_general | solution.py:53
  76.6 5.7 %all-to-all-start.1 = ((bf16[512,8,352]{0,2,1:T(8,128)(2,1)}), bf16[512,8,352]{0,2,1:T(8,128)(2,1)S(1)}, u32[]{:S(2)}, u32[]{:S(2)}) async-start(bf16[512,8,352]{0,2,1:T(8,128)(2,1)} %tile.4), calls=%async_computation.1 | async-start | bytes 5767168 | tf_op jit(solution)/shard_map/all_to_all | solution.py:67
  82.3 10.8 %all_gather.40 = bf16[256,256]{1,0:T(8,128)(2,1)} all-gather(bf16[64,256]{1,0:T(8,128)(2,1)S(1)} %pad_maximum_fusion.5), channel_id=1, replica_groups=mesh['fs_0'=8,'fs_1'=4,'tp'=8] {'fs_1'}, dimensions={0}, use_global_device_ids=true | all-gather | bytes 163840 | tf_op jit(solution)/shard_map/all_gather | solution.py:32
  93.1 13.5 %all-gather.8.cloned.1.call-done = bf16[2816,256]{1,0:T(8,128)(2,1)} async-done(((bf16[352,256]{1,0:T(8,128)(2,1)}), bf16[2816,256]{1,0:T(8,128)(2,1)}) %all-gather.8.cloned.1.call-update) | async-done | bytes 1441808 | tf_op jit(solution)/shard_map/all_gather | solution.py:32
  106.6 10.3 %all-to-all-done.1 = bf16[512,8,352]{0,2,1:T(8,128)(2,1)S(1)} async-done(((bf16[512,8,352]{0,2,1:T(8,128)(2,1)}), bf16[512,8,352]{0,2,1:T(8,128)(2,1)S(1)}, u32[]{:S(2)}, u32[]{:S(2)}) %all-to-all-start.1) | async-done | bytes 2883616 | tf_op jit(solution)/shard_map/all_to_all | solution.py:67
  120.9 4.6 %all-to-all-start.2 = ((bf16[8,512,256]{1,2,0:T(8,128)(2,1)}), bf16[8,512,256]{1,2,0:T(8,128)(2,1)S(1)}, u32[]{:S(2)}, u32[]{:S(2)}) async-start(bf16[8,512,256]{1,2,0:T(8,128)(2,1)} %broadcast_in_dim.9), calls=%async_computation.2 | async-start | bytes 4194304 | tf_op jit(solution)/shard_map/all_to_all | solution.py:15
  125.6 11.4 %all_gather.44 = bf16[256,704]{1,0:T(8,128)(2,1)} all-gather(bf16[64,704]{1,0:T(8,128)(2,1)S(1)} %pad_maximum_fusion.4), channel_id=1, replica_groups=mesh['fs_0'=8,'fs_1'=4,'tp'=8] {'fs_1'}, dimensions={0}, use_global_device_ids=true | all-gather | bytes 450560 | tf_op jit(solution)/shard_map/all_gather | solution.py:32
  137.1 14.6 %all-to-all-done.2 = bf16[8,512,256]{1,2,0:T(8,128)(2,1)S(1)} async-done(((bf16[8,512,256]{1,2,0:T(8,128)(2,1)}), bf16[8,512,256]{1,2,0:T(8,128)(2,1)S(1)}, u32[]{:S(2)}, u32[]{:S(2)}) %all-to-all-start.2) | async-done | bytes 2097184 | tf_op jit(solution)/shard_map/all_to_all | solution.py:15
  159.0 4.9 %slice.212 = f32[4,64,128]{1,2,0:T(8,128)S(1)} slice(f32[4,128,128]{1,2,0:T(8,128)S(1)} %get-tuple-element.6), slice={[0:4:1], [0:127:2], [0:128:1]} | slice | bytes 262144 | tf_op jit(solution)/shard_map/slice | solution.py:114
  164.0 4.5 %slice.213 = f32[4,64,128]{1,2,0:T(8,128)S(1)} slice(f32[4,128,128]{1,2,0:T(8,128)S(1)} %get-tuple-element.6), slice={[0:4:1], [1:128:2], [0:128:1]} | slice | bytes 262144 | tf_op jit(solution)/shard_map/slice | solution.py:114
  168.5 4.5 %slice.211 = f32[4,64,128]{1,2,0:T(8,128)S(1)} slice(f32[4,128,128]{1,2,0:T(8,128)S(1)} %get-tuple-element.5), slice={[0:4:1], [1:128:2], [0:128:1]} | slice | bytes 262144 | tf_op jit(solution)/shard_map/slice | solution.py:114
  173.1 4.5 %slice.215 = f32[4,64,128]{1,2,0:T(8,128)S(1)} slice(f32[4,128,128]{1,2,0:T(8,128)S(1)} %get-tuple-element.5), slice={[0:4:1], [0:127:2], [0:128:1]} | slice | bytes 262144 | tf_op jit(solution)/shard_map/slice | solution.py:114
  221.7 4.5 %slice.259 = f32[4,63,128]{1,2,0:T(8,128)S(1)} slice(f32[4,128,128]{1,2,0:T(8,128)S(1)} %get-tuple-element.6), slice={[0:4:1], [2:128:2], [0:128:1]} | slice | bytes 258048 | tf_op jit(solution)/shard_map/slice | solution.py:114
  226.2 4.5 %slice.210 = f32[4,63,128]{1,2,0:T(8,128)S(1)} slice(f32[4,128,128]{1,2,0:T(8,128)S(1)} %get-tuple-element.5), slice={[0:4:1], [2:128:2], [0:128:1]} | slice | bytes 258048 | tf_op jit(solution)/shard_map/slice | solution.py:114
  252.5 4.6 %pad.61 = f32[4,128,128]{1,2,0:T(8,128)S(1)} pad(f32[4,64,128]{1,2,0:T(8,128)S(1)} %add.195, f32[]{:T(128)} %constant.10.clone.1), padding=0_0_0x1_0_1x0_0_0 | pad | bytes 393220 | tf_op jit(solution)/shard_map/pad | solution.py:114
  257.3 4.5 %pad.60 = f32[4,128,128]{1,2,0:T(8,128)S(1)} pad(f32[4,64,128]{1,2,0:T(8,128)S(1)} %pad_maximum_fusion.2, f32[]{:T(128)} %constant.10.clone.1), padding=0_0_0x0_1_1x0_0_0 | pad | bytes 393220 | tf_op jit(solution)/shard_map/pad | solution.py:114
  263.4 4.6 %all-to-all-start.3 = ((bf16[8,512,128]{1,2,0:T(8,128)(2,1)}), bf16[8,512,128]{1,2,0:T(8,128)(2,1)S(1)}, u32[]{:S(2)}, u32[]{:S(2)}) async-start(bf16[8,512,128]{1,2,0:T(8,128)(2,1)} %broadcast_in_dim.10), calls=%async_computation.3 | async-start | bytes 2097152 | tf_op jit(solution)/shard_map/all_to_all | solution.py:15
  267.9 10.3 %all_gather.42 = bf16[128,256]{1,0:T(8,128)(2,1)S(1)} all-gather(bf16[32,256]{1,0:T(8,128)(2,1)S(1)} %convert_element_type.142), channel_id=1, replica_groups=mesh['fs_0'=8,'fs_1'=4,'tp'=8] {'fs_1'}, dimensions={0}, use_global_device_ids=true | all-gather | bytes 81920 | tf_op jit(solution)/shard_map/all_gather | solution.py:32
  278.2 19.7 %all_gather.43 = bf16[1024,256]{1,0:T(8,128)(2,1)S(1)} all-gather(bf16[128,256]{1,0:T(8,128)(2,1)S(1)} %all_gather.42), channel_id=1, replica_groups=mesh['fs_0'=8,'fs_1'=4,'tp'=8] {'fs_0'}, dimensions={0}, use_global_device_ids=true | all-gather | bytes 589824 | tf_op jit(solution)/shard_map/all_gather | solution.py:32
  300.7 12.7 %all-to-all-start.4 = ((bf16[8,512,256]{1,2,0:T(8,128)(2,1)}), bf16[8,512,256]{1,2,0:T(8,128)(2,1)S(1)}, u32[]{:S(2)}, u32[]{:S(2)}) async-start(bf16[8,512,256]{1,2,0:T(8,128)(2,1)} %broadcast_in_dim.11), calls=%async_computation.4 | async-start | bytes 4194304 | tf_op jit(solution)/shard_map/all_to_all | solution.py:15
  313.4 10.3 %all_gather.46 = bf16[352,256]{1,0:T(8,128)(2,1)} all-gather(bf16[88,256]{1,0:T(8,128)(2,1)S(1)} %convert_element_type.151), channel_id=1, replica_groups=mesh['fs_0'=8,'fs_1'=4,'tp'=8] {'fs_1'}, dimensions={0}, use_global_device_ids=true | all-gather | bytes 225280 | tf_op jit(solution)/shard_map/all_gather | solution.py:32
  323.8 15.8 %all-to-all-done.4 = bf16[8,512,256]{1,2,0:T(8,128)(2,1)S(1)} async-done(((bf16[8,512,256]{1,2,0:T(8,128)(2,1)}), bf16[8,512,256]{1,2,0:T(8,128)(2,1)S(1)}, u32[]{:S(2)}, u32[]{:S(2)}) %all-to-all-start.4) | async-done | bytes 2097184 | tf_op jit(solution)/shard_map/all_to_all | solution.py:15
  342.0 4.3 %fusion.58 = f32[512,704]{0,1:T(8,128)S(1)} fusion(bf16[512,2048]{0,1:T(8,128)(2,1)} %fusion.1, bf16[2048,704]{1,0:T(8,128)(2,1)} %all-gather.12.cloned.1.call-done), kind=kOutput, calls=%fused_computation.112 | convolution fusion | flops 1476395008 | bytes 6422528 | tf_op jit(solution)/shard_map/dot_general | solution.py:53
  348.3 4.5 %all-to-all-start.5 = ((bf16[512,8,352]{0,2,1:T(8,128)(2,1)}), bf16[512,8,352]{0,2,1:T(8,128)(2,1)S(1)}, u32[]{:S(2)}, u32[]{:S(2)}) async-start(bf16[512,8,352]{0,2,1:T(8,128)(2,1)} %tile.5), calls=%async_computation.5 | async-start | bytes 5767168 | tf_op jit(solution)/shard_map/all_to_all | solution.py:67
  352.7 6.4 %all-gather.14.cloned.1.call-done = bf16[2816,256]{1,0:T(8,128)(2,1)} async-done(((bf16[352,256]{1,0:T(8,128)(2,1)}), bf16[2816,256]{1,0:T(8,128)(2,1)}) %all-gather.14.cloned.1.call-update) | async-done | bytes 1441808 | tf_op jit(solution)/shard_map/all_gather | solution.py:32
  359.1 28.2 %all-to-all-done.5 = bf16[512,8,352]{0,2,1:T(8,128)(2,1)S(1)} async-done(((bf16[512,8,352]{0,2,1:T(8,128)(2,1)}), bf16[512,8,352]{0,2,1:T(8,128)(2,1)S(1)}, u32[]{:S(2)}, u32[]{:S(2)}) %all-to-all-start.5) | async-done | bytes 2883616 | tf_op jit(solution)/shard_map/all_to_all | solution.py:67
  387.4 3.0 fusion.11
  (187 shorter events, 94.8 us)
Async XLA Ops:
  6.5 63.8 %all-gather.6.cloned.1.call-start = ((), (), s32[]{:S(2)}) async-start(), calls=%async_computation.6 | async-start | bytes 3538944 | tf_op jit(solution)/shard_map/all_gather | solution.py:32
  23.4 8.2 %copy-start.9 = (f32[88,256]{1,0:T(8,128)S(1)}, f32[88,256]{1,0:T(8,128)}, u32[]{:S(2)}) copy-start(f32[88,256]{1,0:T(8,128)} %param.22) | copy-start | bytes 270340
  23.4 34.4 %all-to-all-start = ((bf16[8,512,256]{1,2,0:T(8,128)(2,1)}), bf16[8,512,256]{1,2,0:T(8,128)(2,1)S(1)}, u32[]{:S(2)}, u32[]{:S(2)}) async-start(bf16[8,512,256]{1,2,0:T(8,128)(2,1)} %broadcast_in_dim.8), calls=%async_computation | async-start | bytes 4194304 | tf_op jit(solution)/shard_map/all_to_all | solution.py:15
  31.5 26.8 %copy-start.14 = (f32[2048]{0:T(1024)S(1)}, f32[2048]{0:T(1024)}, u32[]{:S(2)}) copy-start(f32[2048]{0:T(1024)} %param.19) | copy-start | bytes 24580
  31.5 75.1 %all-gather.8.cloned.1.call-start = ((), (), s32[]{:S(2)}) async-start(), calls=%async_computation.7 | async-start | bytes 1622016 | tf_op jit(solution)/shard_map/all_gather | solution.py:32
  76.6 5.7 %copy-start.11 = (f32[64,128]{1,0:T(8,128)S(1)}, f32[64,128]{1,0:T(8,128)}, u32[]{:S(2)}) copy-start(f32[64,128]{1,0:T(8,128)} %param.24) | copy-start | bytes 98308
  76.6 5.7 %copy-start.12 = (f32[64,128]{1,0:T(8,128)S(1)}, f32[64,128]{1,0:T(8,128)}, u32[]{:S(2)}) copy-start(f32[64,128]{1,0:T(8,128)} %param.25) | copy-start | bytes 98308
  76.6 40.3 %copy-start.2 = (bf16[512,256]{1,0:T(8,128)(2,1)S(1)}, bf16[512,256]{1,0:T(8,128)(2,1)}, u32[]{:S(2)}) copy-start(bf16[512,256]{1,0:T(8,128)(2,1)} %param.18) | copy-start | bytes 786436
  76.6 40.3 %all-to-all-start.1 = ((bf16[512,8,352]{0,2,1:T(8,128)(2,1)}), bf16[512,8,352]{0,2,1:T(8,128)(2,1)S(1)}, u32[]{:S(2)}, u32[]{:S(2)}) async-start(bf16[512,8,352]{0,2,1:T(8,128)(2,1)} %tile.4), calls=%async_computation.1 | async-start | bytes 5767168 | tf_op jit(solution)/shard_map/all_to_all | solution.py:67
  82.2 71.9 %all-gather.10.cloned.1.call-start = ((), (), s32[]{:S(2)}) async-start(), calls=%async_computation.8 | async-start | bytes 1179648 | tf_op jit(solution)/shard_map/all_gather | solution.py:32
  119.2 1.7 copy-start.3
  120.8 4.6 %copy-start.7 = (f32[64,352]{1,0:T(8,128)S(1)}, f32[64,352]{1,0:T(8,128)}, u32[]{:S(2)}) copy-start(f32[64,352]{1,0:T(8,128)} %param.33) | copy-start | bytes 270340
  120.8 4.7 %copy-start.8 = (f32[64,352]{1,0:T(8,128)S(1)}, f32[64,352]{1,0:T(8,128)}, u32[]{:S(2)}) copy-start(f32[64,352]{1,0:T(8,128)} %param.34) | copy-start | bytes 270340
  120.8 16.2 %copy-start.21 = (f32[128]{0:T(128)S(1)}, f32[128]{0:T(128)}, u32[]{:S(2)}) copy-start(f32[128]{0:T(128)} %param.29) | copy-start | bytes 1540
  120.8 16.3 %copy-start.18 = (f32[4,128]{1,0:T(4,128)S(1)}, f32[4,128]{1,0:T(4,128)}, u32[]{:S(2)}) copy-start(f32[4,128]{1,0:T(4,128)} %param.26) | copy-start | bytes 6148
  120.9 30.9 %all-to-all-start.2 = ((bf16[8,512,256]{1,2,0:T(8,128)(2,1)}), bf16[8,512,256]{1,2,0:T(8,128)(2,1)S(1)}, u32[]{:S(2)}, u32[]{:S(2)}) async-start(bf16[8,512,256]{1,2,0:T(8,128)(2,1)} %broadcast_in_dim.9), calls=%async_computation.2 | async-start | bytes 4194304 | tf_op jit(solution)/shard_map/all_to_all | solution.py:15
  125.5 26.8 %copy-start.15 = (f32[2048]{0:T(1024)S(1)}, f32[2048]{0:T(1024)}, u32[]{:S(2)}) copy-start(f32[2048]{0:T(1024)} %param.23) | copy-start | bytes 24580
  125.5 216.5 %all-gather.12.cloned.1.call-start = ((), (), s32[]{:S(2)}) async-start(), calls=%async_computation.9 | async-start | bytes 3538944 | tf_op jit(solution)/shard_map/all_gather | solution.py:32
  154.1 3.9 copy-start.19
  156.8 1.6 copy-start.20
  238.7 7.2 %copy-start.5 = (f32[4,15,128]{1,2,0:T(8,128)S(1)}, f32[4,15,128]{1,2,0:T(8,128)}, u32[]{:S(2)}) copy-start(f32[4,15,128]{1,2,0:T(8,128)} %slice.222) | copy-start | bytes 92164
  238.7 7.2 %copy-start.6 = (f32[4,15,128]{1,2,0:T(8,128)S(1)}, f32[4,15,128]{1,2,0:T(8,128)}, u32[]{:S(2)}) copy-start(f32[4,15,128]{1,2,0:T(8,128)} %slice.255) | copy-start | bytes 92164
  257.1 4.9 %copy-start.1 = (f32[512,256]{1,0:T(8,128)S(1)}, f32[512,256]{1,0:T(8,128)}, u32[]{:S(2)}) copy-start(f32[512,256]{1,0:T(8,128)} %copy-done) | copy-start | bytes 1572868
  262.0 5.9 %copy-start.13 = (f32[32,256]{1,0:T(8,128)S(1)}, f32[32,256]{1,0:T(8,128)}, u32[]{:S(2)}) copy-start(f32[32,256]{1,0:T(8,128)} %param.31) | copy-start | bytes 98308
  263.4 34.9 %copy-start.17 = (f32[1024]{0:T(1024)S(1)}, f32[1024]{0:T(1024)}, u32[]{:S(2)}) copy-start(f32[1024]{0:T(1024)} %param.30) | copy-start | bytes 12292
  263.4 34.6 %all-to-all-start.3 = ((bf16[8,512,128]{1,2,0:T(8,128)(2,1)}), bf16[8,512,128]{1,2,0:T(8,128)(2,1)S(1)}, u32[]{:S(2)}, u32[]{:S(2)}) async-start(bf16[8,512,128]{1,2,0:T(8,128)(2,1)} %broadcast_in_dim.10), calls=%async_computation.3 | async-start | bytes 2097152 | tf_op jit(solution)/shard_map/all_to_all | solution.py:15
  267.9 30.6 %copy-start.4 = (bf16[512,256]{1,0:T(8,128)(2,1)S(1)}, bf16[512,256]{1,0:T(8,128)(2,1)}, u32[]{:S(2)}) copy-start(bf16[512,256]{1,0:T(8,128)(2,1)} %copy-done.3) | copy-start | bytes 786436
  300.7 12.7 %copy-start.10 = (f32[88,256]{1,0:T(8,128)S(1)}, f32[88,256]{1,0:T(8,128)}, u32[]{:S(2)}) copy-start(f32[88,256]{1,0:T(8,128)} %param.35) | copy-start | bytes 270340
  300.7 38.9 %all-to-all-start.4 = ((bf16[8,512,256]{1,2,0:T(8,128)(2,1)}), bf16[8,512,256]{1,2,0:T(8,128)(2,1)S(1)}, u32[]{:S(2)}, u32[]{:S(2)}) async-start(bf16[8,512,256]{1,2,0:T(8,128)(2,1)} %broadcast_in_dim.11), calls=%async_computation.4 | async-start | bytes 4194304 | tf_op jit(solution)/shard_map/all_to_all | solution.py:15
  313.4 26.7 %copy-start.16 = (f32[2048]{0:T(1024)S(1)}, f32[2048]{0:T(1024)}, u32[]{:S(2)}) copy-start(f32[2048]{0:T(1024)} %param.32) | copy-start | bytes 24580
  313.4 45.8 %all-gather.14.cloned.1.call-start = ((), (), s32[]{:S(2)}) async-start(), calls=%async_computation.10 | async-start | bytes 1622016 | tf_op jit(solution)/shard_map/all_gather | solution.py:32
  348.3 39.1 %all-to-all-start.5 = ((bf16[512,8,352]{0,2,1:T(8,128)(2,1)}), bf16[512,8,352]{0,2,1:T(8,128)(2,1)S(1)}, u32[]{:S(2)}, u32[]{:S(2)}) async-start(bf16[512,8,352]{0,2,1:T(8,128)(2,1)} %tile.5), calls=%async_computation.5 | async-start | bytes 5767168 | tf_op jit(solution)/shard_map/all_to_all | solution.py:67
  (1 other events, 0.8 us)
Sparse Core Ops, SparseCore 0:
  20.9 49.3 all-gather.5
  72.1 34.4 all-gather.7
  108.4 36.5 all-gather.9
  146.7 47.1 all-gather.11
  323.9 35.2 all-gather.13
